TPU v7x, 32 devices: a whole 2x2x4 slice. The times are simulated.
32 devices in a mesh: fs: 16 (over z, y, x), tp: 2 (over core).
Axes of the slice: x: 2, y: 2, z: 4, core: 2. Of those that a mesh axis runs over, the one named last changes fastest.
Arguments:
- x_late: bfloat16 [4096, 2048], P('fs'), may hold values from -6 to 6
- x_early: bfloat16 [4096, 2048], P('fs'), may hold values from -6 to 6
- cotangent: bfloat16 [4096, 2048], P('fs'), may hold values from -6 to 6
- w_gate: bfloat16 [2048, 4096], P('fs', 'tp'), may hold values from -0.125 to 0.125
- w_up: bfloat16 [2048, 4096], P('fs', 'tp'), may hold values from -0.125 to 0.125
- w_down: bfloat16 [4096, 2048], P('tp', 'fs'), may hold values from -0.09375 to 0.09375
- conv_taps: float32 [3, 4096], replicated, may hold values from -3 to 3
- conv_bias: float32 [4096], replicated, may hold values from -3 to 3
- grad_down: float32 [4096, 2048], P('tp', 'fs'), may hold values from -60 to 60
Outputs:
- y_late: bfloat16 [4096, 2048], P('fs')
- dx_early: bfloat16 [4096, 2048], P('fs')
- grad_down_out: float32 [4096, 2048], P('tp', 'fs')
All inputs are finite; a program needn't handle non-finite values.
Results may differ from a plain program's by a relative error of at most 0.017.
Values may be sent and summed in bfloat16 or wider, within the bound.
A program may use at most 128 MiB of HBM per device.

v0:
```python
import jax
import jax.numpy as jnp
from jax import lax
from jax.sharding import PartitionSpec as P


def shift_later(field, steps):
    pad = jnp.zeros((steps, field.shape[1]), jnp.float32)
    return jnp.concatenate([pad, field[: field.shape[0] - steps]], axis=0)


def shift_earlier(field, steps):
    pad = jnp.zeros((steps, field.shape[1]), jnp.float32)
    return jnp.concatenate([field[steps:], pad], axis=0)


def contract_last(left, right):
    return lax.dot_general(
        left, right, (((1,), (1,)), ((), ())), preferred_element_type=jnp.float32
    )


def hidden_parts(inputs, gate_full, up_full, taps, bias):
    gate = (
        jnp.dot(inputs, gate_full, preferred_element_type=jnp.float32)
        .astype(jnp.bfloat16)
        .astype(jnp.float32)
    )
    up = jnp.dot(inputs, up_full, preferred_element_type=jnp.float32)
    conv = bias + taps[2] * gate + taps[1] * shift_later(gate, 1) + taps[0] * shift_later(gate, 2)
    act = jax.nn.silu(conv)
    hidden = (act * up).astype(jnp.bfloat16)
    return (conv, act, up, hidden)


def forward_pass(x_late, gate_full, up_full, down_full, taps, bias):
    conv, act, up, hidden = hidden_parts(x_late, gate_full, up_full, taps, bias)
    partial_value = jnp.dot(hidden, down_full, preferred_element_type=jnp.float32)
    return lax.psum(partial_value.astype(jnp.bfloat16), "tp")


def backward_pass(x_early, cotangent, gate_full, up_full, down_full, taps, bias, grad_down):
    conv, act, up, hidden = hidden_parts(x_early, gate_full, up_full, taps, bias)
    dhidden = contract_last(cotangent, down_full)
    summed = lax.psum_scatter(
        lax.dot_general(
            cotangent, hidden, (((0,), (0,)), ((), ())), preferred_element_type=jnp.float32
        ),
        "fs",
        scatter_dimension=0,
        tiled=True,
    )
    grad_down_out = grad_down + summed.T
    dup = (dhidden * act).astype(jnp.bfloat16)
    sig = jax.nn.sigmoid(conv)
    dconv = dhidden * up * sig * (1.0 + conv * (1.0 - sig))
    dgate = taps[2] * dconv + taps[1] * shift_earlier(dconv, 1) + taps[0] * shift_earlier(dconv, 2)
    dgate = dgate.astype(jnp.bfloat16)
    partial_value = contract_last(dup, up_full) + contract_last(dgate, gate_full)
    dx_early = lax.psum(partial_value.astype(jnp.bfloat16), "tp")
    return (dx_early, grad_down_out)


def shards(x_late, x_early, cotangent, w_gate, w_up, w_down, conv_taps, conv_bias, grad_down):
    width = w_gate.shape[1]
    offset = lax.axis_index("tp") * width
    taps = lax.dynamic_slice_in_dim(conv_taps, offset, width, 1)
    bias = lax.dynamic_slice_in_dim(conv_bias, offset, width, 0)
    gate_full, up_full = (
        lax.all_gather(w_gate, "fs", axis=0, tiled=True),
        lax.all_gather(w_up, "fs", axis=0, tiled=True),
    )
    down_full = lax.all_gather(w_down, "fs", axis=1, tiled=True)
    y_late = forward_pass(x_late, gate_full, up_full, down_full, taps, bias)
    dx_early, grad_down_out = backward_pass(
        x_early, cotangent, gate_full, up_full, down_full, taps, bias, grad_down
    )
    return (y_late, dx_early, grad_down_out)


def solution(mesh):
    placed = (
        P("fs", None),
        P("fs", None),
        P("fs", None),
        P("fs", "tp"),
        P("fs", "tp"),
        P("tp", "fs"),
        P(),
        P(),
        P("tp", "fs"),
    )
    return jax.shard_map(
        shards,
        mesh=mesh,
        in_specs=placed,
        out_specs=(P("fs", None), P("fs", None), P("tp", "fs")),
        check_vma=False,
    )
```

profile of v0, /device:TPU:0, one launch (start us, length us, event | category | flops | bytes accessed | tf_op | source)
XLA Modules:
  0.0 786.5 jit_solution(6254999555990808073)
XLA Ops:
  7.2 0.0 copy-start
  7.2 0.0 all-gather.4.cloned.1.call-start
  7.2 0.7 all-gather.4.cloned.1.call-update
  7.9 0.0 all-gather.6.cloned.1.call-start
  8.0 0.7 all-gather.6.cloned.1.call-update
  8.7 0.0 all-gather.8.cloned.1.call-start
  8.7 0.7 all-gather.8.cloned.1.call-update
  9.4 0.0 reduce-scatter.2.cloned.1.call-start
  9.4 0.7 dynamic_slice.6
  10.2 1.0 fusion.16
  11.1 0.0 copy-start.7
  11.1 114.7 %all-gather.4.cloned.1.call-done = bf16[2048,2048]{1,0:T(8,128)(2,1)} async-done(((bf16[128,2048]{1,0:T(8,128)(2,1)}), bf16[2048,2048]{1,0:T(8,128)(2,1)}) %all-gather.4.cloned.1.call-update) | async-done | bytes 8388624 | tf_op jit(solution)/shard_map/all_gather | solution.py:70
  125.8 7.4 fusion.2
  133.2 105.9 %all-gather.6.cloned.1.call-done = bf16[2048,2048]{1,0:T(8,128)(2,1)} async-done(((bf16[128,2048]{1,0:T(8,128)(2,1)}), bf16[2048,2048]{1,0:T(8,128)(2,1)}) %all-gather.6.cloned.1.call-update) | async-done | bytes 8388624 | tf_op jit(solution)/shard_map/all_gather | solution.py:71
  239.1 0.0 copy-done.7
  239.1 7.1 fusion.17
  246.2 135.7 %all-gather.8.cloned.1.call-done = bf16[2048,2048]{1,0:T(8,128)(2,1)} async-done(((bf16[2048,128]{1,0:T(8,128)(2,1)}), bf16[2048,2048]{1,0:T(8,128)(2,1)}) %all-gather.8.cloned.1.call-update) | async-done | bytes 8388624 | tf_op jit(solution)/shard_map/all_gather | solution.py:73
  381.8 0.0 copy-done
  381.8 0.0 copy-start.4
  381.8 10.6 %add_multiply_fusion = (f32[256,2048]{1,0:T(8,128)S(1)}, f32[256,2048]{1,0:T(8,128)S(1)}, f32[256,2048]{1,0:T(8,128)}) fusion(f32[256,2048]{1,0:T(8,128)} %fusion.17, f32[254,2048]{1,0:T(8,128)} %bitcast.38, f32[2048]{0:T(1024)S(1)} %bitcast.31, f32[255,2048]{1,0:T(8,128)} %bitcast.39, f32[2048]{0:T(1024)S(1)} %bitcast.28, f32[256,2048]{1,0:T(8,128)} %fusion.2, ...), kind=kOutput, calls=%fused_computation.12 | convolution fusion | flops 2155347968 | bytes 24125440 | tf_op jit(solution)/shard_map/dot_general | solution.py:18
  392.5 0.0 copy-start.2
  392.5 1.3 copy-done.2
  393.8 0.0 copy-done.4
  393.8 8.2 %convolution_bitcast_fusion = f32[2048,2048]{0,1:T(8,128)} fusion(bf16[256,2048]{1,0:T(8,128)(2,1)S(1)} %copy-done, f32[256,2048]{1,0:T(8,128)S(1)} %copy-done.4, f32[256,2048]{1,0:T(8,128)S(1)} %get-tuple-element.6), kind=kOutput, calls=%fused_computation | convolution fusion | flops 2150629376 | bytes 22020096 | tf_op jit(solution)/shard_map/dot_general | solution.py:46
  402.0 0.0 reduce-scatter.2.cloned.1.call-update
  402.0 0.2 all-reduce.9.cloned.1.call-start
  402.2 0.0 copy-start.8
  402.2 0.2 slice.47
  402.4 0.0 slice-start
  402.4 0.2 slice.46
  402.6 0.8 copy-done.8
  403.5 0.0 copy-start.3
  403.5 0.0 copy-start.9
  403.5 0.0 slice-start.1
  403.5 8.4 %fusion.3 = f32[256,2048]{1,0:T(8,128)} fusion(bf16[256,2048]{1,0:T(8,128)(2,1)S(1)} %copy-done.8, bf16[2048,2048]{1,0:T(8,128)(2,1)} %all-gather.4.cloned.1.call-done), kind=kOutput, calls=%fused_computation.9 | convolution fusion | flops 2148532224 | bytes 11534336 | tf_op jit(solution)/shard_map/dot_general | solution.py:25
  411.8 0.0 copy-done.3
  411.8 0.0 copy-done.9
  411.8 7.2 fusion.5
  419.0 0.0 slice-done
  419.0 0.0 slice-done.1
  419.0 5.1 fusion
  424.1 13.8 %convolution_convert_fusion.1 = bf16[256,2048]{1,0:T(8,128)(2,1)} fusion(bf16[2048,2048]{1,0:T(8,128)(2,1)} %all-gather.8.cloned.1.call-done, bf16[256,2048]{1,0:T(8,128)(2,1)S(1)} %copy-done.8, bf16[2048,2048]{1,0:T(8,128)(2,1)} %all-gather.6.cloned.1.call-done, f32[254,2048]{1,0:T(8,128)} %bitcast.36, f32[255,2048]{1,0:T(8,128)} %bitcast.37, ...), kind=kOutput, calls=%fused_computation.7 | convolution fusion | flops 4301783040 | bytes 25174016 | tf_op jit(solution)/shard_map/dot_general | solution.py:38
  437.9 0.0 copy-start.5
  437.9 0.0 all-reduce.9.cloned.1.call-update
  437.9 308.8 %reduce-scatter.2.cloned.1.call-done = f32[128,2048]{0,1:T(8,128)} async-done(((f32[2048,2048]{0,1:T(8,128)}), f32[128,2048]{0,1:T(8,128)}) %reduce-scatter.2.cloned.1.call-update) | async-done | bytes 1048592 | tf_op jit(solution)/shard_map/reduce_scatter | solution.py:45
  746.8 0.0 copy-done.5
  746.8 2.3 bitcast_add_fusion
  749.1 27.5 %all-reduce.9.cloned.1.call-done = (bf16[256,2048]{1,0:T(8,128)(2,1)}, bf16[256,2048]{1,0:T(8,128)(2,1)}) async-done(((bf16[256,2048]{1,0:T(8,128)(2,1)}, bf16[256,2048]{1,0:T(8,128)(2,1)}), (bf16[256,2048]{1,0:T(8,128)(2,1)}, bf16[256,2048]{1,0:T(8,128)(2,1)})) %all-reduce.9.cloned.1.call-update) | async-done | bytes 2097168 | tf_op jit(solution)/shard_map/psum | solution.py:39
  776.6 0.0 copy-start.6
  776.6 0.0 copy-start.1
  776.6 2.5 copy.14
  779.0 0.0 copy-done.6
  779.0 1.0 copy.15
  780.0 0.0 copy-done.1
  (1 shorter events, 0.0 us)
Async XLA Ops:
  7.2 374.7 %copy-start = (bf16[256,2048]{1,0:T(8,128)(2,1)S(1)}, bf16[256,2048]{1,0:T(8,128)(2,1)}, u32[]{:S(2)}) copy-start(bf16[256,2048]{1,0:T(8,128)(2,1)} %param.11) | copy-start | bytes 3145732
  7.2 118.6 %all-gather.4.cloned.1.call-start = ((), (), s32[]{:S(2)}) async-start(), calls=%async_computation.1 | async-start | bytes 8912896 | tf_op jit(solution)/shard_map/all_gather | solution.py:70
  7.9 231.2 %all-gather.6.cloned.1.call-start = ((), (), s32[]{:S(2)}) async-start(), calls=%async_computation.2 | async-start | bytes 8912896 | tf_op jit(solution)/shard_map/all_gather | solution.py:71
  8.7 373.2 %all-gather.8.cloned.1.call-start = ((), (), s32[]{:S(2)}) async-start(), calls=%async_computation.3 | async-start | bytes 8912896 | tf_op jit(solution)/shard_map/all_gather | solution.py:73
  9.4 737.4 %reduce-scatter.2.cloned.1.call-start = ((), (), s32[]{:S(2)}) async-start(), calls=%async_computation.4 | async-start | bytes 17825792 | tf_op jit(solution)/shard_map/reduce_scatter | solution.py:45
  11.1 228.0 %copy-start.7 = (bf16[256,2048]{1,0:T(8,128)(2,1)S(1)}, bf16[256,2048]{1,0:T(8,128)(2,1)}, u32[]{:S(2)}) copy-start(bf16[256,2048]{1,0:T(8,128)(2,1)} %param.10) | copy-start | bytes 3145732
  381.8 11.9 %copy-start.4 = (f32[256,2048]{1,0:T(8,128)S(1)}, f32[256,2048]{1,0:T(8,128)}, u32[]{:S(2)}) copy-start(f32[256,2048]{1,0:T(8,128)} %fusion.17) | copy-start | bytes 6291460
  392.5 1.3 copy-start.2
  402.0 374.6 %all-reduce.9.cloned.1.call-start = ((), (), s32[]{:S(2)}) async-start(), calls=%async_computation.5 | async-start | bytes 4194304 | tf_op jit(solution)/shard_map/psum | solution.py:39
  402.2 1.2 copy-start.8
  402.4 16.6 %slice-start = ((s8[8388608]{0:T(1024)(128)(4,1)}), s8[4194304]{0:T(1024)(128)(4,1)S(1)}, s32[]{:S(2)}) async-start(s8[8388608]{0:T(1024)(128)(4,1)} %bitcast.34), calls=%async_computation.6 | async-start | bytes 8388608
  403.5 8.4 %copy-start.3 = (f32[256,2048]{1,0:T(8,128)S(1)}, f32[256,2048]{1,0:T(8,128)}, u32[]{:S(2)}) copy-start(f32[256,2048]{1,0:T(8,128)} %copy-done.2) | copy-start | bytes 6291460
  403.5 8.4 %copy-start.9 = (f32[256,2048]{1,0:T(8,128)S(1)}, f32[256,2048]{1,0:T(8,128)}, u32[]{:S(2)}) copy-start(f32[256,2048]{1,0:T(8,128)} %get-tuple-element.10) | copy-start | bytes 6291460
  403.5 15.5 %slice-start.1 = ((s8[8388608]{0:T(1024)(128)(4,1)}), s8[4194304]{0:T(1024)(128)(4,1)S(1)}, s32[]{:S(2)}) async-start(s8[8388608]{0:T(1024)(128)(4,1)} %bitcast.34), calls=%async_computation.7 | async-start | bytes 8388608
  437.9 308.8 %copy-start.5 = (f32[2048,128]{1,0:T(8,128)S(1)}, f32[2048,128]{1,0:T(8,128)}, u32[]{:S(2)}) copy-start(f32[2048,128]{1,0:T(8,128)} %param.17) | copy-start | bytes 3145732
  776.6 2.5 copy-start.6
  776.6 3.4 copy-start.1
Sparse Core Ops, SparseCore 0:
  10.8 115.0 all-gather.3
  128.6 110.4 all-gather.5
  241.8 139.9 all-gather.7
  402.1 344.5 reduce-scatter.1
  749.6 26.9 all-reduce.8
where the time goes:
time: 787 us
  waiting for transfers between devices  695 us (88%)
  matrix products  67.7 us (9%)
  between operations  13.9 us (2%)
    reduce_scatter x1, waiting for transfers between devices, backward_pass(): lax.psum_scatter(lax.dot_general(cotangent, hidden, (((0,), (0,)), ((), (...  309 us
    all_gather x1, waiting for transfers between devices, shards(): down_full = lax.all_gather(w_down, 'fs', axis=1, tiled=True)  136 us
    all_gather x1, waiting for transfers between devices, shards(): lax.all_gather(w_gate, 'fs', axis=0, tiled=True)  115 us
    all_gather x1, waiting for transfers between devices, shards(): lax.all_gather(w_up, 'fs', axis=0, tiled=True)  106 us
    psum x1, waiting for transfers between devices, forward_pass(): return lax.psum(partial_value.astype(jnp.bfloat16), 'tp')  27.5 us
    dot_general x3, matrix products, contract_last(): lax.dot_general(left, right, (((1,), (1,)), ((), ())), preferred_element_...  22.9 us
    dot_general x2, matrix products, hidden_parts(): jnp.dot(inputs, gate_full, preferred_element_type=jnp.float32)  15.7 us
  transfers between devices with their start and end apart: 5, of which 5 were waited for; matrix products, arithmetic and copies ran while one was open for 7% of the time, Pallas kernels for 0%

commit v1 on v0

--- a/solution.py
+++ b/solution.py
@@ -1,7 +1,315 @@
+import functools
+
 import jax
 import jax.numpy as jnp
 from jax import lax
+from jax.experimental import pallas as pl
+from jax.experimental.pallas import tpu as pltpu
 from jax.sharding import PartitionSpec as P
+
+GROUP = 4
+VMEM_BYTES = 60 * 1024 * 1024
+ANY = pl.BlockSpec(memory_space=pl.ANY)
+VMEM = pl.BlockSpec(memory_space=pltpu.VMEM)
+
+
+def place():
+    f, c = lax.axis_index("fs"), lax.axis_index("tp")
+    q, z = lax.rem(f, GROUP), lax.div(f, GROUP)
+    qx = q + 1 - 2 * lax.rem(q, 2)
+    qy = q + 2 - 4 * lax.div(q, 2)
+    qa, qb = qx + c * (qy - qx), qy + c * (qx - qy)
+    return f, c, q, z, qa, qb, GROUP - 1 - q
+
+
+def at(start, size):
+    return pl.ds(pl.multiple_of(start, size), size)
+
+
+def remote(src, dst, send, recv, **device):
+    return pltpu.make_async_remote_copy(
+        src_ref=src, dst_ref=dst, send_sem=send, recv_sem=recv,
+        device_id=device, device_id_type=pl.DeviceIdType.MESH,
+    )
+
+
+def gather_kernel(nz, x0, x1, x2, wg, wu, wd, t0, t1, t2, og, ou, od,
+                  loc, w_s, w_r, n_s, n_r, p_s, p_r, r_s, r_r, l_s, l_r):
+    f, c, q, z, qa, qb, qd = place()
+    base = z * GROUP
+    xs, ts, outs = (x0, x1, x2), (t0, t1, t2), (og, ou, od)
+    rows = x0.shape[0]
+    half = rows // 2
+    r, u = wg.shape[0], og.shape[1]
+    first, last = z > 0, z < nz - 1
+
+    barrier = pltpu.get_barrier_semaphore()
+    for peer in (qa, qb, qd):
+        pl.semaphore_signal(barrier, 1, device_id={"fs": base + peer}, device_id_type=pl.DeviceIdType.MESH)
+    pl.semaphore_signal(barrier, 1, device_id={"tp": 1 - c}, device_id_type=pl.DeviceIdType.MESH)
+
+    for s in range(1, nz):
+        pl.semaphore_signal(barrier, 1, device_id={"fs": lax.rem(z + s, nz) * GROUP + q},
+                            device_id_type=pl.DeviceIdType.MESH)
+    pl.semaphore_wait(barrier, 3 + nz)
+
+    def piece(k, peer):
+        if k == 2:
+            return wd.at[at(peer * u, u), :]
+        return (wg, wu)[k].at[:, at(peer * u, u)]
+
+    def landing(k, owner):
+        if k == 2:
+            return od.at[:, at(owner * r, r)]
+        return outs[k].at[at(owner * r, r), :]
+
+    weights = []
+    for k in range(3):
+        for d, peer in enumerate((qa, qb, qd)):
+            copy = remote(piece(k, peer), landing(k, f), w_s.at[k, d], w_r.at[k, d], fs=base + peer)
+            copy.start()
+            weights.append(copy)
+    mine = at(c * half, half)
+    near = []
+    for i in range(3):
+        for d, peer in enumerate((qa, qb)):
+            copy = remote(xs[i].at[mine, :], ts[i].at[q, mine, :], n_s.at[i, d], n_r.at[i, d], fs=base + peer)
+            copy.start()
+            near.append(copy)
+    local = []
+    for k in range(3):
+        copy = pltpu.make_async_copy(piece(k, q), landing(k, f), loc.at[k])
+        copy.start()
+        local.append(copy)
+    for i in range(3):
+        copy = pltpu.make_async_copy(xs[i], ts[i].at[q], loc.at[3 + i])
+        copy.start()
+        local.append(copy)
+
+    def block(k, b):
+        if k == 2:
+            return od.at[:, at(b * GROUP * r, GROUP * r)]
+        return outs[k].at[at(b * GROUP * r, GROUP * r), :]
+
+    def right(k, s):
+        b = block(k, z - s)
+        return remote(b, b, r_s.at[s, k], r_r.at[s, k], fs=f + GROUP)
+
+    def left(k, s):
+        b = block(k, z + s)
+        return remote(b, b, l_s.at[s, k], l_r.at[s, k], fs=f - GROUP)
+
+    def arrived(k, s):
+        @pl.when(z - s - 1 >= 0)
+        def _():
+            b = block(k, z - s - 1)
+            remote(b, b, r_s.at[s, k], r_r.at[s, k], fs=f - GROUP).wait_recv()
+
+        @pl.when(z + s + 1 < nz)
+        def _():
+            b = block(k, z + s + 1)
+            remote(b, b, l_s.at[s, k], l_r.at[s, k], fs=f + GROUP).wait_recv()
+
+    def onward(k, s, act):
+        @pl.when(jnp.logical_and(z - s >= 0, last))
+        def _():
+            act(right(k, s))
+
+        @pl.when(jnp.logical_and(z + s < nz, first))
+        def _():
+            act(left(k, s))
+
+    begin, sent = (lambda copy: copy.start()), (lambda copy: copy.wait_send())
+
+    for k in range(3):
+        local[k].wait()
+        for d in range(3):
+            weights[3 * k + d].wait_recv()
+        onward(k, 0, begin)
+
+    partner = []
+
+    def pass_on(i, owner, kind):
+        there = ts[i].at[owner, mine, :]
+        copy = remote(there, there, p_s.at[i, kind], p_r.at[i, kind], tp=1 - c)
+        copy.start()
+        partner.append((copy, i, owner, kind))
+
+    far = []
+    for i in range(3):
+        near[2 * i].wait_recv()
+        there = ts[i].at[qa, mine, :]
+        copy = remote(there, there, n_s.at[i, 2], n_r.at[i, 2], fs=base + qb)
+        copy.start()
+        far.append(copy)
+        pass_on(i, qa, 0)
+        if nz > 2:
+            arrived(i, 0)
+            onward(i, 1, begin)
+    for i in range(3):
+        near[2 * i + 1].wait_recv()
+        pass_on(i, qb, 1)
+    for i in range(3):
+        far[i].wait_recv()
+        pass_on(i, qd, 2)
+    for s in range(2, nz - 1):
+        for k in range(3):
+            arrived(k, s - 1)
+            onward(k, s, begin)
+    for k in range(3):
+        if nz > 1:
+            arrived(k, nz - 2)
+    other = at((1 - c) * half, half)
+    for copy, i, owner, kind in partner:
+        copy.wait_send()
+        theirs = (qb, qa, qd)[kind]
+        there = ts[i].at[theirs, other, :]
+        remote(there, there, p_s.at[i, kind], p_r.at[i, kind], tp=1 - c).wait_recv()
+    for copy in weights + near + far:
+        copy.wait_send()
+    for copy in local[3:]:
+        copy.wait()
+    for s in range(nz - 1):
+        for k in range(3):
+            onward(k, s, sent)
+
+
+def gather(nz, xs, w_gate, w_up, w_down):
+    rows, d = xs[0].shape
+    units = w_gate.shape[1] // GROUP
+    dma = pltpu.SemaphoreType.DMA
+    hops = max(nz - 1, 1)
+    tok = jax.ShapeDtypeStruct((GROUP, rows, d), xs[0].dtype)
+    col = jax.ShapeDtypeStruct((d, units), w_gate.dtype)
+    row = jax.ShapeDtypeStruct((units, d), w_gate.dtype)
+    return pl.pallas_call(
+        functools.partial(gather_kernel, nz),
+        out_shape=(tok, tok, tok, col, col, row),
+        in_specs=[VMEM] * 6,
+        out_specs=(ANY,) * 6,
+        scratch_shapes=[dma((6,)), dma((3, 3)), dma((3, 3)), dma((3, 3)), dma((3, 3)),
+                        dma((3, 3)), dma((3, 3)), dma((hops, 3)), dma((hops, 3)),
+                        dma((hops, 3)), dma((hops, 3))],
+        compiler_params=pltpu.CompilerParams(collective_id=0, has_side_effects=True, vmem_limit_bytes=VMEM_BYTES),
+        name="gather_group",
+    )(*xs, w_gate, w_up, w_down)
+
+
+def total(dst, srcs, rows, step=16):
+    @pl.loop(0, rows, step=step)
+    def _(i):
+        sl = pl.ds(pl.multiple_of(i, step), step)
+        out = srcs[0][sl, :].astype(jnp.float32)
+        for s in srcs[1:]:
+            out = out + s[sl, :].astype(jnp.float32)
+        dst[sl, :] = out.astype(dst.dtype)
+
+
+def scatter_kernel(nz, yp, xp, gp, y, dx, g, core, summed, got, gin, gsum,
+                   c_s, c_r, a_s, a_r, z_s, z_r, g_s, g_r, e_s, e_r):
+    f, c, q, z, qa, qb, qd = place()
+    base = z * GROUP
+    parts, outs = (yp, xp), (y, dx)
+    rows = y.shape[0]
+    half = rows // 2
+    u = gp.shape[0]
+    r = g.shape[1]
+    wide = GROUP * r
+
+    barrier = pltpu.get_barrier_semaphore()
+    for peer in (qa, qb, qd):
+        pl.semaphore_signal(barrier, 1, device_id={"fs": base + peer}, device_id_type=pl.DeviceIdType.MESH)
+    pl.semaphore_signal(barrier, 1, device_id={"tp": 1 - c}, device_id_type=pl.DeviceIdType.MESH)
+    for s in range(1, nz):
+        pl.semaphore_signal(barrier, 1, device_id={"fs": lax.rem(z + s, nz) * GROUP + q},
+                            device_id_type=pl.DeviceIdType.MESH)
+    pl.semaphore_wait(barrier, 3 + nz)
+
+    order = (qd, qa, qb, q)
+    theirs = (qd, qb, qa, q)
+    cores = []
+    for t in range(2):
+        for n in range(4):
+            src = parts[t].at[at(theirs[n] * rows + (1 - c) * half, half), :]
+            copy = remote(src, core.at[t, n], c_s.at[t, n], c_r.at[t, n], tp=1 - c)
+            copy.start()
+            cores.append(copy)
+    grads = []
+    for s in range(1, nz):
+        to = lax.rem(z + s, nz)
+        copy = remote(gp.at[:, at(to * wide, wide)], gin.at[s], z_s.at[s], z_r.at[s], fs=to * GROUP + q)
+        copy.start()
+        grads.append(copy)
+
+    sends = {}
+
+    def send(t, n, slot, peer):
+        copy = remote(summed.at[t, n], got.at[t, slot], a_s.at[t, slot], a_r.at[t, slot], fs=base + peer)
+        copy.start()
+        sends[t, slot] = copy
+
+    for n in range(4):
+        for t in range(2):
+            cores[4 * t + n].wait_recv()
+            own = parts[t].at[at(order[n] * rows + c * half, half), :]
+            total(summed.at[t, n], [own, core.at[t, n]], half)
+            if n == 0:
+                send(t, 0, 0, qa)
+            if n == 1:
+                send(t, 1, 1, qa)
+    for t in range(2):
+        sends[t, 0].wait_recv()
+        total(core.at[t, 0], [summed.at[t, 2], got.at[t, 0]], half)
+        copy = remote(core.at[t, 0], got.at[t, 2], a_s.at[t, 2], a_r.at[t, 2], fs=base + qb)
+        copy.start()
+        sends[t, 2] = copy
+    for copy in grads:
+        copy.wait_recv()
+    total(gsum, [gp.at[:, at(z * wide, wide)]] + [gin.at[s] for s in range(1, nz)], u)
+    handed = []
+    for d, peer in enumerate((qa, qb, qd)):
+        copy = remote(gsum.at[:, at(peer * r, r)], g.at[at(q * u, u), :], g_s.at[d], g_r.at[d], fs=base + peer)
+        copy.start()
+        handed.append(copy)
+    g[at(q * u, u), :] = gsum[:, at(q * r, r)]
+    ends = []
+    mine = at(c * half, half)
+    for t in range(2):
+        sends[t, 1].wait_recv()
+        sends[t, 2].wait_recv()
+        total(outs[t].at[mine, :], [summed.at[t, 3], got.at[t, 1], got.at[t, 2]], half)
+        copy = remote(outs[t].at[mine, :], outs[t].at[mine, :], e_s.at[t], e_r.at[t], tp=1 - c)
+        copy.start()
+        ends.append(copy)
+    for copy in handed + ends:
+        copy.wait_recv()
+    for copy in cores + grads + handed + ends + list(sends.values()):
+        copy.wait_send()
+
+
+def scatter(nz, y_part, dx_part, g_part):
+    d = y_part.shape[1]
+    rows = y_part.shape[0] // GROUP
+    u = g_part.shape[0]
+    r = d // (nz * GROUP)
+    half = rows // 2
+    dma = pltpu.SemaphoreType.DMA
+    b16 = jnp.bfloat16
+    out = jax.ShapeDtypeStruct((rows, d), b16)
+    return pl.pallas_call(
+        functools.partial(scatter_kernel, nz),
+        out_shape=(out, out, jax.ShapeDtypeStruct((u * GROUP, r), b16)),
+        in_specs=[VMEM] * 3,
+        out_specs=(VMEM,) * 3,
+        scratch_shapes=[
+            pltpu.VMEM((2, 4, half, d), b16), pltpu.VMEM((2, 4, half, d), b16), pltpu.VMEM((2, 3, half, d), b16),
+            pltpu.VMEM((nz, u, GROUP * r), b16), pltpu.VMEM((u, GROUP * r), b16),
+            dma((2, 4)), dma((2, 4)), dma((2, 3)), dma((2, 3)), dma((nz,)), dma((nz,)),
+            dma((3,)), dma((3,)), dma((2,)), dma((2,)),
+        ],
+        compiler_params=pltpu.CompilerParams(collective_id=1, has_side_effects=True, vmem_limit_bytes=VMEM_BYTES),
+        name="scatter_group",
+    )(y_part, dx_part, g_part)
 
 
 def shift_later(field, steps):
@@ -9,6 +317,16 @@
     return jnp.concatenate([pad, field[: field.shape[0] - steps]], axis=0)
 
 
+def seq_later(field, steps, rows):
+    row = lax.rem(lax.broadcasted_iota(jnp.int32, (field.shape[0], 1), 0), rows)
+    return jnp.where(row >= steps, shift_later(field, steps), 0.0)
+
+
+def seq_earlier(field, steps, rows):
+    row = lax.rem(lax.broadcasted_iota(jnp.int32, (field.shape[0], 1), 0), rows)
+    return jnp.where(row < rows - steps, shift_earlier(field, steps), 0.0)
+
+
 def shift_earlier(field, steps):
     pad = jnp.zeros((steps, field.shape[1]), jnp.float32)
     return jnp.concatenate([field[steps:], pad], axis=0)
@@ -20,27 +338,27 @@
     )
 
 
-def hidden_parts(inputs, gate_full, up_full, taps, bias):
+def hidden_parts(inputs, gate_full, up_full, taps, bias, rows):
     gate = (
         jnp.dot(inputs, gate_full, preferred_element_type=jnp.float32)
         .astype(jnp.bfloat16)
         .astype(jnp.float32)
     )
     up = jnp.dot(inputs, up_full, preferred_element_type=jnp.float32)
-    conv = bias + taps[2] * gate + taps[1] * shift_later(gate, 1) + taps[0] * shift_later(gate, 2)
+    conv = bias + taps[2] * gate + taps[1] * seq_later(gate, 1, rows) + taps[0] * seq_later(gate, 2, rows)
     act = jax.nn.silu(conv)
     hidden = (act * up).astype(jnp.bfloat16)
     return (conv, act, up, hidden)
 
 
 def forward_pass(x_late, gate_full, up_full, down_full, taps, bias):
-    conv, act, up, hidden = hidden_parts(x_late, gate_full, up_full, taps, bias)
+    conv, act, up, hidden = hidden_parts(x_late, gate_full, up_full, taps, bias, x_late.shape[0])
     partial_value = jnp.dot(hidden, down_full, preferred_element_type=jnp.float32)
     return lax.psum(partial_value.astype(jnp.bfloat16), "tp")
 
 
 def backward_pass(x_early, cotangent, gate_full, up_full, down_full, taps, bias, grad_down):
-    conv, act, up, hidden = hidden_parts(x_early, gate_full, up_full, taps, bias)
+    conv, act, up, hidden = hidden_parts(x_early, gate_full, up_full, taps, bias, x_early.shape[0])
     dhidden = contract_last(cotangent, down_full)
     summed = lax.psum_scatter(
         lax.dot_general(
@@ -78,7 +396,44 @@
     return (y_late, dx_early, grad_down_out)
 
 
+def grouped_shards(nz, x_late, x_early, cotangent, w_gate, w_up, w_down, conv_taps, conv_bias, grad_down):
+    rows, d = x_late.shape
+    units = w_gate.shape[1] // GROUP
+    start = (lax.axis_index("tp") * GROUP + lax.rem(lax.axis_index("fs"), GROUP)) * units
+    taps = lax.dynamic_slice_in_dim(conv_taps, start, units, 1)
+    bias = lax.dynamic_slice_in_dim(conv_bias, start, units, 0)
+    late, early, cot, gate_w, up_w, down_w = gather(nz, (x_late, x_early, cotangent), w_gate, w_up, w_down)
+    late, early, cot = (t.reshape(GROUP * rows, d) for t in (late, early, cot))
+
+    hidden = hidden_parts(late, gate_w, up_w, taps, bias, rows)[3]
+    y_part = jnp.dot(hidden, down_w, preferred_element_type=jnp.float32).astype(jnp.bfloat16)
+
+    conv, act, up, hidden = hidden_parts(early, gate_w, up_w, taps, bias, rows)
+    g_part = lax.dot_general(
+        hidden, cot, (((0,), (0,)), ((), ())), preferred_element_type=jnp.float32
+    ).astype(jnp.bfloat16)
+    dhidden = contract_last(cot, down_w)
+    dup = (dhidden * act).astype(jnp.bfloat16)
+    sig = jax.nn.sigmoid(conv)
+    dconv = dhidden * up * sig * (1.0 + conv * (1.0 - sig))
+    dgate = taps[2] * dconv + taps[1] * seq_earlier(dconv, 1, rows) + taps[0] * seq_earlier(dconv, 2, rows)
+    dgate = dgate.astype(jnp.bfloat16)
+    dx_part = (contract_last(dup, up_w) + contract_last(dgate, gate_w)).astype(jnp.bfloat16)
+
+    y_late, dx_early, grad = scatter(nz, y_part, dx_part, g_part)
+    return (y_late, dx_early, grad_down + grad.astype(jnp.float32))
+
+
 def solution(mesh):
+    def step(*arrays):
+        x_late, w_gate = arrays[0], arrays[3]
+        fs, tp = mesh.shape["fs"], mesh.shape["tp"]
+        units, rest = divmod(w_gate.shape[1], GROUP)
+        lanes_ok = rest == 0 and units % 128 == 0 and w_gate.shape[0] % 128 == 0
+        if tp == 2 and fs % GROUP == 0 and lanes_ok and x_late.shape[0] % 32 == 0:
+            return grouped_shards(fs // GROUP, *arrays)
+        return shards(*arrays)
+
     placed = (
         P("fs", None),
         P("fs", None),
@@ -91,7 +446,7 @@
         P("tp", "fs"),
     )
     return jax.shard_map(
-        shards,
+        step,
         mesh=mesh,
         in_specs=placed,
         out_specs=(P("fs", None), P("fs", None), P("tp", "fs")),

time: 787 us -> 223 us (0.28)
  the two profiles are of different devices: /device:TPU:0 before, /device:TPU:8 now
where the time goes in v1:
time: 223 us; the launch traced here: 222 us
  Pallas kernels  175 us (78%)
  matrix products  40.1 us (18%)
  local copies, waits for them, and re-layouts  4.64 us (2%)
  other arithmetic  2.25 us (1%)
    pallas_call x1, Pallas kernels, gather(): pl.pallas_call(functools.partial(gather_kernel, nz), out_shape=(tok, tok,...  115 us
    pallas_call x1, Pallas kernels, scatter(): pl.pallas_call(functools.partial(scatter_kernel, nz), out_shape=(out, out...  59.3 us
    dot_general x1, matrix products, grouped_shards(): jnp.dot(hidden, down_w, preferred_element_type=jnp.float32)  11.7 us
    dot_general x2, matrix products, hidden_parts(): jnp.dot(inputs, gate_full, preferred_element_type=jnp.float32)  11.2 us
    dot_general x3, matrix products, contract_last(): lax.dot_general(left, right, (((1,), (1,)), ((), ())), preferred_element_...  10.8 us

profile of v1, /device:TPU:8, one launch (start us, length us, event | category | flops | bytes accessed | tf_op | source)
XLA Modules:
  0.0 222.3 jit_solution(887789669857185247)
XLA Ops:
  0.6 0.8 dynamic_slice.6
  1.4 0.9 fusion.21
  2.3 115.2 %gather_group.1 = (bf16[4,256,2048]{2,1,0:T(8,128)(2,1)}, bf16[4,256,2048]{2,1,0:T(8,128)(2,1)}, bf16[4,256,2048]{2,1,0:T(8,128)(2,1)}, bf16[2048,512]{1,0:T(8,1...) custom-call(bf16[256,2048]{1,0:T(8,128)(2,1)} %x0.1, bf16[256,2048]{1,0:T(8,128)(2,1)} %x1.1, ...), custom_call_target="tpu_custom_call" | custom-call | tf_op jit(solution)/shard_map/gather_group/pallas_call | solution.py:185
  117.5 6.5 %fusion.2 = f32[1024,512]{1,0:T(8,128)} fusion(bf16[1024,2048]{1,0:T(8,128)(2,1)} %bitcast.37, bf16[2048,512]{1,0:T(8,128)(2,1)} %get-tuple-element.13), kind=kOutput, calls=%fused_computation.14 | convolution fusion | flops 2148532224 | bytes 8388608 | tf_op jit(solution)/shard_map/dot_general | solution.py:343
  124.0 0.0 copy-start
  124.0 11.7 %convolution_convert_fusion.yp = bf16[1024,2048]{1,0:T(8,128)(2,1)} fusion(bf16[512,2048]{1,0:T(8,128)(2,1)} %get-tuple-element.15, f32[1022,512]{1,0:T(8,128)} %bitcast.41, f32[1023,512]{1,0:T(8,128)} %bitcast.42, f32[1024,512]{1,0:T(8,128)} %fusion.2, bf16[1024,2048]{1,0:T(8,128)(2,1)} %bitcast.38, bf16[2048,512]{1,0:T(8,128)(2,1)} %get-tuple-element.14, ...), kind=kOutput, calls=%fused_computation.1 | convolution fusion | flops 4304404480 | bytes 18878464 | tf_op jit(solution)/shard_map/dot_general | solution.py:409
  135.8 0.0 copy-done
  135.8 0.0 copy-start.5
  135.8 0.0 copy-start.6
  135.8 4.7 %fusion.1 = f32[1024,512]{1,0:T(8,128)S(1)} fusion(bf16[1024,2048]{1,0:T(8,128)(2,1)} %bitcast.35, bf16[2048,512]{1,0:T(8,128)(2,1)S(1)} %copy-done), kind=kOutput, calls=%fused_computation.12 | convolution fusion | flops 2148532224 | bytes 8388608 | tf_op jit(solution)/shard_map/dot_general | solution.py:343
  140.5 0.0 copy-done.5
  140.5 0.0 copy-done.6
  140.5 0.0 copy-start.4
  140.5 0.0 copy-start.7
  140.5 2.3 %fusion.22 = f32[1024,512]{1,0:T(8,128)S(1)} fusion(bf16[1024,2048]{1,0:T(8,128)(2,1)S(1)} %bitcast.36, bf16[2048,512]{1,0:T(8,128)(2,1)S(1)} %copy-done.6), kind=kOutput, calls=%fused_computation.35 | convolution fusion | flops 2147483648 | bytes 8388608 | tf_op jit(solution)/shard_map/dot_general | solution.py:347
  142.8 0.0 copy-done.4
  142.8 0.5 copy-done.7
  143.3 3.7 %add_multiply_fusion = (f32[1024,512]{1,0:T(8,128)S(1)}, f32[1024,512]{1,0:T(8,128)S(1)}, f32[1024,512]{1,0:T(8,128)S(1)}) fusion(f32[1024,512]{1,0:T(8,128)S(1)} %fusion.22, f32[1022,512]{1,0:T(8,128)S(1)} %bitcast.39, pred[1024]{0:T(1024)(128)(4,1)S(1)} %get-tuple-element.27, f32[512]{0:T(512)S(1)} %bitcast.31, f32[1023,512]{1,0:T(8,128)S(1)} %bitcast.40, ...), kind=kOutput, calls=%fused_computation.5 | convolution fusion | flops 2156396544 | bytes 20975616 | tf_op jit(solution)/shard_map/dot_general | solution.py:336
  147.0 4.0 %convolution_convert_fusion.1.gp = bf16[512,2048]{1,0:T(8,128)(2,1)} fusion(bf16[1024,2048]{1,0:T(8,128)(2,1)S(1)} %bitcast.34, f32[1024,512]{1,0:T(8,128)S(1)} %fusion.22, f32[1024,512]{1,0:T(8,128)S(1)} %get-tuple-element.22), kind=kOutput, calls=%fused_computation.2 | convolution fusion | flops 2151677952 | bytes 10485760 | tf_op jit(solution)/shard_map/dot_general | solution.py:412
  151.1 2.4 %fusion.3 = f32[1024,2048]{1,0:T(8,128)S(1)} fusion(bf16[2048,512]{1,0:T(8,128)(2,1)S(1)} %copy-done.6, f32[1024,512]{1,0:T(8,128)S(1)} %get-tuple-element.26, f32[1024,512]{1,0:T(8,128)S(1)} %get-tuple-element.22), kind=kOutput, calls=%fused_computation.15 | convolution fusion | flops 2150629376 | bytes 14680064 | tf_op jit(solution)/shard_map/dot_general | solution.py:336
  153.5 0.3 slice.47
  153.7 0.3 slice.46
  154.0 4.7 %add_convert_fusion.xp = bf16[1024,2048]{1,0:T(8,128)(2,1)} fusion(f32[1024,2048]{1,0:T(8,128)S(1)} %fusion.3, bf16[2048,512]{1,0:T(8,128)(2,1)S(1)} %copy-done, f32[1022,512]{1,0:T(8,128)S(1)} %slice.47, f32[1023,512]{1,0:T(8,128)S(1)} %slice.46, f32[1024,512]{1,0:T(8,128)S(1)} %get-tuple-element.21, f32[512]{0:T(512)S(1)} %bitcast.32, f32[512]{0:T(512)S(1)} %bitcast.29, ...), kind=kOutput, calls=%fused_computation | convolution fusion | flops 2155872256 | bytes 20973568 | tf_op jit(solution)/shard_map/dot_general | solution.py:336
  158.7 0.0 copy-start.1
  158.7 59.3 %scatter_group.1 = (bf16[256,2048]{1,0:T(8,128)(2,1)}, bf16[256,2048]{1,0:T(8,128)(2,1)}, bf16[2048,128]{1,0:T(8,128)(2,1)}) custom-call(bf16[1024,2048]{1,0:T(8,128)(2,1)} %convolution_convert_fusion.yp, bf16[1024,2048]{1,0:T(8,128)(2,1)} %add_convert_fusion.xp, bf16[512,2048]{1,0:T(8,128)(2,1)} %convolution_convert_fusion.1.gp), custom_call_target="tpu_custom_call" | custom-call | tf_op jit(solution)/shard_map/scatter_group/pallas_call | solution.py:299
  218.1 0.0 copy-start.3
  218.1 0.0 copy-done.1
  218.1 0.0 copy-start.2
  218.1 2.2 %convert_add_fusion = f32[2048,128]{1,0:T(8,128)} fusion(f32[2048,128]{1,0:T(8,128)S(1)} %copy-done.1, bf16[2048,128]{1,0:T(8,128)(2,1)} %get-tuple-element.20), kind=kLoop, calls=%fused_computation.16 | loop fusion | flops 524288 | bytes 2621440 | tf_op jit(solution)/shard_map/add | solution.py:424
  220.3 0.0 copy-done.3
  220.3 1.0 copy.14
  221.3 0.0 copy-done.2
  221.3 1.0 copy.15
  (2 shorter events, 0.0 us)
Async XLA Ops:
  124.0 11.7 %copy-start = (bf16[2048,512]{1,0:T(8,128)(2,1)S(1)}, bf16[2048,512]{1,0:T(8,128)(2,1)}, u32[]{:S(2)}) copy-start(bf16[2048,512]{1,0:T(8,128)(2,1)} %get-tuple-element.13) | copy-start | bytes 6291460
  135.8 4.7 %copy-start.5 = (bf16[4,256,2048]{2,1,0:T(8,128)(2,1)S(1)}, bf16[4,256,2048]{2,1,0:T(8,128)(2,1)}, u32[]{:S(2)}) copy-start(bf16[4,256,2048]{2,1,0:T(8,128)(2,1)} %get-tuple-element.17) | copy-start | bytes 12582916
  135.8 4.7 %copy-start.6 = (bf16[2048,512]{1,0:T(8,128)(2,1)S(1)}, bf16[2048,512]{1,0:T(8,128)(2,1)}, u32[]{:S(2)}) copy-start(bf16[2048,512]{1,0:T(8,128)(2,1)} %get-tuple-element.14) | copy-start | bytes 6291460
  140.5 2.4 %copy-start.4 = (bf16[4,256,2048]{2,1,0:T(8,128)(2,1)S(1)}, bf16[4,256,2048]{2,1,0:T(8,128)(2,1)}, u32[]{:S(2)}) copy-start(bf16[4,256,2048]{2,1,0:T(8,128)(2,1)} %get-tuple-element.16) | copy-start | bytes 12582916
  140.5 2.9 %copy-start.7 = (bf16[512,2048]{1,0:T(8,128)(2,1)S(1)}, bf16[512,2048]{1,0:T(8,128)(2,1)}, u32[]{:S(2)}) copy-start(bf16[512,2048]{1,0:T(8,128)(2,1)} %get-tuple-element.15) | copy-start | bytes 6291460
  158.7 59.4 %copy-start.1 = (f32[2048,128]{1,0:T(8,128)S(1)}, f32[2048,128]{1,0:T(8,128)}, u32[]{:S(2)}) copy-start(f32[2048,128]{1,0:T(8,128)} %param.17) | copy-start | bytes 3145732
  218.1 2.3 %copy-start.3 = (bf16[256,2048]{1,0:T(8,128)(2,1)S(1)}, bf16[256,2048]{1,0:T(8,128)(2,1)}, u32[]{:S(2)}) copy-start(bf16[256,2048]{1,0:T(8,128)(2,1)} %get-tuple-element.34) | copy-start | bytes 3145732
  218.1 3.2 %copy-start.2 = (bf16[256,2048]{1,0:T(8,128)(2,1)S(1)}, bf16[256,2048]{1,0:T(8,128)(2,1)}, u32[]{:S(2)}) copy-start(bf16[256,2048]{1,0:T(8,128)(2,1)} %get-tuple-element.35) | copy-start | bytes 3145732

commit v2 on v1

v2 whole, which is shorter than its diff:
```python
import functools

import jax
import jax.numpy as jnp
from jax import lax
from jax.experimental import pallas as pl
from jax.experimental.pallas import tpu as pltpu
from jax.sharding import PartitionSpec as P

GROUP = 4
VMEM_BYTES = 60 * 1024 * 1024
VMEM = pl.BlockSpec(memory_space=pltpu.VMEM)


def place():
    f, c = lax.axis_index("fs"), lax.axis_index("tp")
    q, z = lax.rem(f, GROUP), lax.div(f, GROUP)
    qx = q + 1 - 2 * lax.rem(q, 2)
    qy = q + 2 - 4 * lax.div(q, 2)
    qa, qb = qx + c * (qy - qx), qy + c * (qx - qy)
    return f, c, q, z, qa, qb, GROUP - 1 - q


def at(start, size):
    return pl.ds(pl.multiple_of(start, size), size)


def remote(src, dst, send, recv, **device):
    return pltpu.make_async_remote_copy(
        src_ref=src, dst_ref=dst, send_sem=send, recv_sem=recv,
        device_id=device, device_id_type=pl.DeviceIdType.MESH,
    )


def total(dst, srcs, rows, step=16):
    @pl.loop(0, rows, step=step)
    def _(i):
        sl = pl.ds(pl.multiple_of(i, step), step)
        out = srcs[0][sl, :].astype(jnp.float32)
        for s in srcs[1:]:
            out = out + s[sl, :].astype(jnp.float32)
        dst[sl, :] = out.astype(dst.dtype)


def mm(left, right, dims=((1,), (0,))):
    return lax.dot_general(left, right, (dims, ((), ())), preferred_element_type=jnp.float32)


def layer_kernel(nz, tile, x0, x1, x2, wg, wu, wd, taps, bias, y, dx, g,
                 t0, t1, t2, og, ou, od, hid, hid_t, conv_s, up_s, dup, dgate, yp, xp, gp,
                 core, summed, got, gin, gsum,
                 loc, w_s, w_r, n_s, n_r, p_s, p_r, r_s, r_r, l_s, l_r,
                 c_s, c_r, a_s, a_r, z_s, z_r, g_s, g_r, e_s, e_r):
    f, c, q, z, qa, qb, qd = place()
    base = z * GROUP
    xs, ts, outs = (x0, x1, x2), (t0, t1, t2), (og, ou, od)
    rows, d_model = x0.shape
    half = rows // 2
    r, u = wg.shape[0], og.shape[1]
    wide = GROUP * r
    first, last = z > 0, z < nz - 1

    barrier = pltpu.get_barrier_semaphore()
    for peer in (qa, qb, qd):
        pl.semaphore_signal(barrier, 1, device_id={"fs": base + peer}, device_id_type=pl.DeviceIdType.MESH)
    pl.semaphore_signal(barrier, 1, device_id={"tp": 1 - c}, device_id_type=pl.DeviceIdType.MESH)

    for s in range(1, nz):
        pl.semaphore_signal(barrier, 1, device_id={"fs": lax.rem(z + s, nz) * GROUP + q},
                            device_id_type=pl.DeviceIdType.MESH)
    pl.semaphore_wait(barrier, 3 + nz)

    def piece(k, peer):
        if k == 2:
            return wd.at[at(peer * u, u), :]
        return (wg, wu)[k].at[:, at(peer * u, u)]

    def landing(k, owner):
        if k == 2:
            return od.at[:, at(owner * r, r)]
        return outs[k].at[at(owner * r, r), :]

    weights = []
    for k in range(3):
        for d, peer in enumerate((qa, qb, qd)):
            copy = remote(piece(k, peer), landing(k, f), w_s.at[k, d], w_r.at[k, d], fs=base + peer)
            copy.start()
            weights.append(copy)
    mine = at(c * half, half)
    near = []
    for i in range(3):
        for d, peer in enumerate((qa, qb)):
            copy = remote(xs[i].at[mine, :], ts[i].at[q, mine, :], n_s.at[i, d], n_r.at[i, d], fs=base + peer)
            copy.start()
            near.append(copy)
    local = []
    for k in range(3):
        copy = pltpu.make_async_copy(piece(k, q), landing(k, f), loc.at[k])
        copy.start()
        local.append(copy)
    for i in range(3):
        copy = pltpu.make_async_copy(xs[i], ts[i].at[q], loc.at[3 + i])
        copy.start()
        local.append(copy)

    def block(k, b):
        if k == 2:
            return od.at[:, at(b * GROUP * r, GROUP * r)]
        return outs[k].at[at(b * GROUP * r, GROUP * r), :]

    def right(k, s):
        b = block(k, z - s)
        return remote(b, b, r_s.at[s, k], r_r.at[s, k], fs=f + GROUP)

    def left(k, s):
        b = block(k, z + s)
        return remote(b, b, l_s.at[s, k], l_r.at[s, k], fs=f - GROUP)

    def arrived(k, s):
        @pl.when(z - s - 1 >= 0)
        def _():
            b = block(k, z - s - 1)
            remote(b, b, r_s.at[s, k], r_r.at[s, k], fs=f - GROUP).wait_recv()

        @pl.when(z + s + 1 < nz)
        def _():
            b = block(k, z + s + 1)
            remote(b, b, l_s.at[s, k], l_r.at[s, k], fs=f + GROUP).wait_recv()

    def onward(k, s, act):
        @pl.when(jnp.logical_and(z - s >= 0, last))
        def _():
            act(right(k, s))

        @pl.when(jnp.logical_and(z + s < nz, first))
        def _():
            act(left(k, s))

    begin, sent = (lambda copy: copy.start()), (lambda copy: copy.wait_send())

    row = lax.broadcasted_iota(jnp.int32, (rows, tile), 0)

    def later(v, steps):
        return jnp.where(row >= steps, pltpu.roll(v, steps, 0), 0.0)

    def earlier(v, steps):
        return jnp.where(row < rows - steps, pltpu.roll(v, rows - steps, 0), 0.0)

    def forward(t, keep):
        @pl.loop(0, GROUP)
        def _(b):
            @pl.loop(0, u // tile)
            def _(j):
                cols, seq = at(j * tile, tile), at(b * rows, rows)
                x = t[b]
                gate = mm(x, og[:, cols]).astype(jnp.bfloat16).astype(jnp.float32)
                up = mm(x, ou[:, cols])
                conv = (bias[:, cols] + taps[2:3, cols] * gate + taps[1:2, cols] * later(gate, 1)
                        + taps[0:1, cols] * later(gate, 2))
                out = conv / (1.0 + jnp.exp(-conv)) * up
                if keep:
                    conv_s[seq, cols] = conv
                    up_s[seq, cols] = up
                    hid_t[at(j * tile, tile), seq] = out.T.astype(jnp.bfloat16)
                else:
                    hid[seq, cols] = out.astype(jnp.bfloat16)

    def down_grad():
        @pl.loop(0, d_model // tile)
        def _(j):
            cols = at(j * tile, tile)
            cot = t2[:, :, cols].reshape(GROUP * rows, tile)
            gp[:, cols] = mm(hid_t[...], cot).astype(jnp.bfloat16)

    def backward():
        @pl.loop(0, GROUP)
        def _(b):
            @pl.loop(0, u // tile)
            def _(j):
                cols, seq = at(j * tile, tile), at(b * rows, rows)
                dh = mm(t2[b], od[at(j * tile, tile), :], ((1,), (1,)))
                conv = conv_s[seq, cols]
                sig = 1.0 / (1.0 + jnp.exp(-conv))
                dup[seq, cols] = (dh * (conv * sig)).astype(jnp.bfloat16)
                dc = dh * up_s[seq, cols] * sig * (1.0 + conv * (1.0 - sig))
                dg = (taps[2:3, cols] * dc + taps[1:2, cols] * earlier(dc, 1)
                      + taps[0:1, cols] * earlier(dc, 2))
                dgate[seq, cols] = dg.astype(jnp.bfloat16)

    def late_out(owner):
        seq = at(owner * rows, rows)

        @pl.loop(0, d_model // tile)
        def _(j):
            cols = at(j * tile, tile)
            yp[seq, cols] = mm(hid[seq, :], od[:, cols]).astype(jnp.bfloat16)

    def early_out(owner):
        seq = at(owner * rows, rows)

        @pl.loop(0, d_model // tile)
        def _(j):
            cols = at(j * tile, tile)
            part = mm(dup[seq, :], ou[cols, :], ((1,), (1,))) + mm(dgate[seq, :], og[cols, :], ((1,), (1,)))
            xp[seq, cols] = part.astype(jnp.bfloat16)

    def enter(k):
        local[k].wait()
        for d in range(3):
            weights[3 * k + d].wait_recv()
        onward(k, 0, begin)

    enter(0)
    enter(1)
    partner = []

    def pass_on(i, owner, kind):
        there = ts[i].at[owner, mine, :]
        copy = remote(there, there, p_s.at[i, kind], p_r.at[i, kind], tp=1 - c)
        copy.start()
        partner.append((copy, i, owner, kind))

    far = []
    for i in range(3):
        near[2 * i].wait_recv()
        there = ts[i].at[qa, mine, :]
        copy = remote(there, there, n_s.at[i, 2], n_r.at[i, 2], fs=base + qb)
        copy.start()
        far.append(copy)
        pass_on(i, qa, 0)
        if i < 2 and nz > 2:
            arrived(i, 0)
            onward(i, 1, begin)
    for i in range(3):
        near[2 * i + 1].wait_recv()
        pass_on(i, qb, 1)
    for s in range(2, nz - 1):
        for k in range(2):
            arrived(k, s - 1)
            onward(k, s, begin)
    enter(2)
    for i in range(3):
        far[i].wait_recv()
        pass_on(i, qd, 2)
    if nz > 1:
        arrived(0, nz - 2)
        arrived(1, nz - 2)
    other = at((1 - c) * half, half)
    for copy, i, owner, kind in partner:
        there = ts[i].at[(qb, qa, qd)[kind], other, :]
        remote(there, there, p_s.at[i, kind], p_r.at[i, kind], tp=1 - c).wait_recv()
    for copy in local[3:]:
        copy.wait()

    jobs = [lambda: forward(t1, True), lambda: forward(t0, False), down_grad]
    for s in range(1, nz - 1):
        if jobs:
            jobs.pop(0)()
        arrived(2, s - 1)
        onward(2, s, begin)
    while jobs:
        jobs.pop(0)()
    grads = []
    for s in range(1, nz):
        to = lax.rem(z + s, nz)
        copy = remote(gp.at[:, at(to * wide, wide)], gin.at[s], z_s.at[s], z_r.at[s], fs=to * GROUP + q)
        copy.start()
        grads.append(copy)
    if nz > 1:
        arrived(2, nz - 2)

    parts, finals = (yp, xp), (y, dx)
    order = (qd, qa, qb, q)
    theirs = (qd, qb, qa, q)
    cores, sends = {}, {}

    def to_core(t, n):
        src = parts[t].at[at(theirs[n] * rows + (1 - c) * half, half), :]
        copy = remote(src, core.at[t, n], c_s.at[t, n], c_r.at[t, n], tp=1 - c)
        copy.start()
        cores[t, n] = copy

    def send(t, n, slot, peer):
        copy = remote(summed.at[t, n], got.at[t, slot], a_s.at[t, slot], a_r.at[t, slot], fs=base + peer)
        copy.start()
        sends[t, slot] = copy

    def join(t, n):
        cores[t, n].wait_recv()
        own = parts[t].at[at(order[n] * rows + c * half, half), :]
        total(summed.at[t, n], [own, core.at[t, n]], half)
        if n == 0:
            send(t, 0, 0, qa)
        if n == 1:
            send(t, 1, 1, qa)

    def onto_second(t):
        sends[t, 0].wait_recv()
        total(core.at[t, 0], [summed.at[t, 2], got.at[t, 0]], half)
        copy = remote(core.at[t, 0], got.at[t, 2], a_s.at[t, 2], a_r.at[t, 2], fs=base + qb)
        copy.start()
        sends[t, 2] = copy

    ends = []

    def finish(t):
        sends[t, 1].wait_recv()
        sends[t, 2].wait_recv()
        total(finals[t].at[mine, :], [summed.at[t, 3], got.at[t, 1], got.at[t, 2]], half)
        there = finals[t].at[mine, :]
        copy = remote(there, there, e_s.at[t], e_r.at[t], tp=1 - c)
        copy.start()
        ends.append(copy)

    def produce(t, make):
        make(qd)
        to_core(t, 0)
        make(qa)
        make(qb)
        to_core(t, 1)
        to_core(t, 2)
        join(t, 0)
        make(q)
        to_core(t, 3)
        for n in (1, 2):
            join(t, n)

    produce(0, late_out)
    backward()
    join(0, 3)
    onto_second(0)
    produce(1, early_out)
    join(1, 3)
    finish(0)
    onto_second(1)
    for copy in grads:
        copy.wait_recv()
    total(gsum, [gp.at[:, at(z * wide, wide)]] + [gin.at[s] for s in range(1, nz)], u)
    handed = []
    for d, peer in enumerate((qa, qb, qd)):
        copy = remote(gsum.at[:, at(peer * r, r)], g.at[at(q * u, u), :], g_s.at[d], g_r.at[d], fs=base + peer)
        copy.start()
        handed.append(copy)
    g[at(q * u, u), :] = gsum[:, at(q * r, r)]
    finish(1)
    for copy in handed + ends:
        copy.wait_recv()
    for copy in weights + near + far + [p[0] for p in partner]:
        copy.wait_send()
    for copy in list(cores.values()) + grads + handed + ends + list(sends.values()):
        copy.wait_send()
    for s in range(nz - 1):
        for k in range(3):
            onward(k, s, sent)


def layer(nz, xs, w_gate, w_up, w_down, taps, bias):
    rows, d = xs[0].shape
    u = w_gate.shape[1] // GROUP
    r = w_gate.shape[0]
    half, toks = rows // 2, GROUP * rows
    tile = 256 if u % 256 == 0 else 128
    sems = lambda *shape: [pltpu.SemaphoreType.DMA(shape)] * 2
    b16, f32 = jnp.bfloat16, jnp.float32
    out = jax.ShapeDtypeStruct((rows, d), b16)
    hops = max(nz - 1, 1)
    return pl.pallas_call(
        functools.partial(layer_kernel, nz, tile),
        out_shape=(out, out, jax.ShapeDtypeStruct((u * GROUP, r), b16)),
        in_specs=[VMEM] * 8,
        out_specs=(VMEM,) * 3,
        scratch_shapes=[pltpu.VMEM((GROUP, rows, d), b16)] * 3
        + [pltpu.VMEM((d, u), b16)] * 2
        + [pltpu.VMEM((u, d), b16), pltpu.VMEM((toks, u), b16), pltpu.VMEM((u, toks), b16),
           pltpu.VMEM((toks, u), f32), pltpu.VMEM((toks, u), f32),
           pltpu.VMEM((toks, u), b16), pltpu.VMEM((toks, u), b16),
           pltpu.VMEM((toks, d), b16), pltpu.VMEM((toks, d), b16), pltpu.VMEM((u, d), b16),
           pltpu.VMEM((2, 4, half, d), b16), pltpu.VMEM((2, 4, half, d), b16), pltpu.VMEM((2, 3, half, d), b16),
           pltpu.VMEM((nz, u, GROUP * r), b16), pltpu.VMEM((u, GROUP * r), b16),
           pltpu.SemaphoreType.DMA((6,))]
        + sems(3, 3) + sems(3, 3) + sems(3, 3) + sems(hops, 3) + sems(hops, 3)
        + sems(2, 4) + sems(2, 3) + sems(nz) + sems(3) + sems(2),
        compiler_params=pltpu.CompilerParams(collective_id=0, has_side_effects=True, vmem_limit_bytes=VMEM_BYTES),
        name="layer_group",
    )(*xs, w_gate, w_up, w_down, taps, bias)


def shift_later(field, steps):
    pad = jnp.zeros((steps, field.shape[1]), jnp.float32)
    return jnp.concatenate([pad, field[: field.shape[0] - steps]], axis=0)


def shift_earlier(field, steps):
    pad = jnp.zeros((steps, field.shape[1]), jnp.float32)
    return jnp.concatenate([field[steps:], pad], axis=0)


def contract_last(left, right):
    return lax.dot_general(
        left, right, (((1,), (1,)), ((), ())), preferred_element_type=jnp.float32
    )


def hidden_parts(inputs, gate_full, up_full, taps, bias):
    gate = (
        jnp.dot(inputs, gate_full, preferred_element_type=jnp.float32)
        .astype(jnp.bfloat16)
        .astype(jnp.float32)
    )
    up = jnp.dot(inputs, up_full, preferred_element_type=jnp.float32)
    conv = bias + taps[2] * gate + taps[1] * shift_later(gate, 1) + taps[0] * shift_later(gate, 2)
    act = jax.nn.silu(conv)
    hidden = (act * up).astype(jnp.bfloat16)
    return (conv, act, up, hidden)


def forward_pass(x_late, gate_full, up_full, down_full, taps, bias):
    conv, act, up, hidden = hidden_parts(x_late, gate_full, up_full, taps, bias)
    partial_value = jnp.dot(hidden, down_full, preferred_element_type=jnp.float32)
    return lax.psum(partial_value.astype(jnp.bfloat16), "tp")


def backward_pass(x_early, cotangent, gate_full, up_full, down_full, taps, bias, grad_down):
    conv, act, up, hidden = hidden_parts(x_early, gate_full, up_full, taps, bias)
    dhidden = contract_last(cotangent, down_full)
    summed = lax.psum_scatter(
        lax.dot_general(
            cotangent, hidden, (((0,), (0,)), ((), ())), preferred_element_type=jnp.float32
        ),
        "fs",
        scatter_dimension=0,
        tiled=True,
    )
    grad_down_out = grad_down + summed.T
    dup = (dhidden * act).astype(jnp.bfloat16)
    sig = jax.nn.sigmoid(conv)
    dconv = dhidden * up * sig * (1.0 + conv * (1.0 - sig))
    dgate = taps[2] * dconv + taps[1] * shift_earlier(dconv, 1) + taps[0] * shift_earlier(dconv, 2)
    dgate = dgate.astype(jnp.bfloat16)
    partial_value = contract_last(dup, up_full) + contract_last(dgate, gate_full)
    dx_early = lax.psum(partial_value.astype(jnp.bfloat16), "tp")
    return (dx_early, grad_down_out)


def shards(x_late, x_early, cotangent, w_gate, w_up, w_down, conv_taps, conv_bias, grad_down):
    width = w_gate.shape[1]
    offset = lax.axis_index("tp") * width
    taps = lax.dynamic_slice_in_dim(conv_taps, offset, width, 1)
    bias = lax.dynamic_slice_in_dim(conv_bias, offset, width, 0)
    gate_full, up_full = (
        lax.all_gather(w_gate, "fs", axis=0, tiled=True),
        lax.all_gather(w_up, "fs", axis=0, tiled=True),
    )
    down_full = lax.all_gather(w_down, "fs", axis=1, tiled=True)
    y_late = forward_pass(x_late, gate_full, up_full, down_full, taps, bias)
    dx_early, grad_down_out = backward_pass(
        x_early, cotangent, gate_full, up_full, down_full, taps, bias, grad_down
    )
    return (y_late, dx_early, grad_down_out)


def grouped_shards(nz, x_late, x_early, cotangent, w_gate, w_up, w_down, conv_taps, conv_bias, grad_down):
    units = w_gate.shape[1] // GROUP
    start = (lax.axis_index("tp") * GROUP + lax.rem(lax.axis_index("fs"), GROUP)) * units
    taps = lax.dynamic_slice_in_dim(conv_taps, start, units, 1)
    bias = lax.dynamic_slice_in_dim(conv_bias, start, units, 0)
    y_late, dx_early, grad = layer(
        nz, (x_late, x_early, cotangent), w_gate, w_up, w_down, taps, bias.reshape(1, units)
    )
    return (y_late, dx_early, grad_down + grad.astype(jnp.float32))


def solution(mesh):
    def step(*arrays):
        x_late, w_gate = arrays[0], arrays[3]
        fs, tp = mesh.shape["fs"], mesh.shape["tp"]
        units, rest = divmod(w_gate.shape[1], GROUP)
        lanes_ok = rest == 0 and units % 128 == 0 and w_gate.shape[0] % 128 == 0
        if tp == 2 and fs % GROUP == 0 and lanes_ok and x_late.shape[0] % 32 == 0:
            return grouped_shards(fs // GROUP, *arrays)
        return shards(*arrays)

    placed = (
        P("fs", None),
        P("fs", None),
        P("fs", None),
        P("fs", "tp"),
        P("fs", "tp"),
        P("tp", "fs"),
        P(),
        P(),
        P("tp", "fs"),
    )
    return jax.shard_map(
        step,
        mesh=mesh,
        in_specs=placed,
        out_specs=(P("fs", None), P("fs", None), P("tp", "fs")),
        check_vma=False,
    )
```

time: 223 us -> 201 us (0.901)
  the two profiles are of different devices: /device:TPU:8 before, /device:TPU:0 now
where the time goes in v2:
time: 201 us
  Pallas kernels  193 us (96%)
  local copies, waits for them, and re-layouts  4.56 us (2%)
  other arithmetic  2.19 us (1%)
    pallas_call x1, Pallas kernels, layer(): pl.pallas_call(functools.partial(layer_kernel, nz, tile), out_shape=(out,...  193 us

profile of v2, /device:TPU:0, one launch (start us, length us, event | category | flops | bytes accessed | tf_op | source)
XLA Modules:
  0.0 200.6 jit_solution(11358447965728112809)
XLA Ops:
  0.6 0.0 copy-start
  0.7 1.4 dynamic_slice.7
  2.0 0.0 copy-done
  2.0 0.6 constant_dynamic-slice_fusion.taps
  2.6 0.0 copy-start.1
  2.6 193.2 %layer_group.1 = (bf16[256,2048]{1,0:T(8,128)(2,1)}, bf16[256,2048]{1,0:T(8,128)(2,1)}, bf16[2048,128]{1,0:T(8,128)(2,1)}) custom-call(bf16[256,2048]{1,0:T(8,128)(2,1)} %x0.1, bf16[256,2048]{1,0:T(8,128)(2,1)} %x1.1, bf16[256,2048]{1,0:T(8,128)(2,1)} %x2.1, bf16[128,2048]{1,0:T(8,128)(2,1)} %wg.1, bf16[128,2048]{1,0:T(8,128)(2,1)} %wu.1, ...), custom_call_target="tpu_custom_call" | custom-call | tf_op jit(solution)/shard_map/layer_group/pallas_call | solution.py:367
  195.8 0.0 copy-done.1
  195.8 0.0 copy-start.3
  195.8 2.2 %convert_add_fusion = f32[2048,128]{1,0:T(8,128)} fusion(f32[2048,128]{1,0:T(8,128)S(1)} %copy-done.1, bf16[2048,128]{1,0:T(8,128)(2,1)} %get-tuple-element.8), kind=kLoop, calls=%fused_computation | loop fusion | flops 524288 | bytes 2621440 | tf_op jit(solution)/shard_map/add | solution.py:470
  198.0 0.0 copy-done.3
  198.0 0.0 copy-start.2
  198.0 1.0 copy.14
  199.0 0.6 copy-done.2
  199.6 1.0 copy.15
Async XLA Ops:
  0.6 1.4 copy-start
  2.6 193.2 %copy-start.1 = (f32[2048,128]{1,0:T(8,128)S(1)}, f32[2048,128]{1,0:T(8,128)}, u32[]{:S(2)}) copy-start(f32[2048,128]{1,0:T(8,128)} %param.17) | copy-start | bytes 3145732
  195.8 2.2 %copy-start.3 = (bf16[256,2048]{1,0:T(8,128)(2,1)S(1)}, bf16[256,2048]{1,0:T(8,128)(2,1)}, u32[]{:S(2)}) copy-start(bf16[256,2048]{1,0:T(8,128)(2,1)} %get-tuple-element.12) | copy-start | bytes 3145732
  198.0 1.6 copy-start.2

commit v3 on v2

--- a/solution.py
+++ b/solution.py
@@ -139,6 +139,8 @@
     begin, sent = (lambda copy: copy.start()), (lambda copy: copy.wait_send())
 
     row = lax.broadcasted_iota(jnp.int32, (rows, tile), 0)
+
+    wide_tile = 2 * tile if d_model % (2 * tile) == 0 else tile
 
     def later(v, steps):
         return jnp.where(row >= steps, pltpu.roll(v, steps, 0), 0.0)
@@ -166,10 +168,10 @@
                     hid[seq, cols] = out.astype(jnp.bfloat16)
 
     def down_grad():
-        @pl.loop(0, d_model // tile)
+        @pl.loop(0, d_model // wide_tile)
         def _(j):
-            cols = at(j * tile, tile)
-            cot = t2[:, :, cols].reshape(GROUP * rows, tile)
+            cols = at(j * wide_tile, wide_tile)
+            cot = t2[:, :, cols].reshape(GROUP * rows, wide_tile)
             gp[:, cols] = mm(hid_t[...], cot).astype(jnp.bfloat16)
 
     def backward():
@@ -190,17 +192,17 @@
     def late_out(owner):
         seq = at(owner * rows, rows)
 
-        @pl.loop(0, d_model // tile)
+        @pl.loop(0, d_model // wide_tile)
         def _(j):
-            cols = at(j * tile, tile)
+            cols = at(j * wide_tile, wide_tile)
             yp[seq, cols] = mm(hid[seq, :], od[:, cols]).astype(jnp.bfloat16)
 
     def early_out(owner):
         seq = at(owner * rows, rows)
 
-        @pl.loop(0, d_model // tile)
+        @pl.loop(0, d_model // wide_tile)
         def _(j):
-            cols = at(j * tile, tile)
+            cols = at(j * wide_tile, wide_tile)
             part = mm(dup[seq, :], ou[cols, :], ((1,), (1,))) + mm(dgate[seq, :], og[cols, :], ((1,), (1,)))
             xp[seq, cols] = part.astype(jnp.bfloat16)
 

time: 201 us -> 198 us (0.985)
  Pallas kernels: 193 us -> 190 us
    pallas_call x1, Pallas kernels: 193 us -> 190 us  [layer(): pl.pallas_call(functools.partial(layer_kernel, nz, tile), out_shape=(out,...]
where the time goes in v3:
time: 198 us
  Pallas kernels  190 us (96%)
  local copies, waits for them, and re-layouts  4.56 us (2%)
  other arithmetic  2.19 us (1%)
    pallas_call x1, Pallas kernels, layer(): pl.pallas_call(functools.partial(layer_kernel, nz, tile), out_shape=(out,...  190 us

profile of v3, /device:TPU:0, one launch (start us, length us, event | category | flops | bytes accessed | tf_op | source)
XLA Modules:
  0.0 197.9 jit_solution(14732989446540928877)
XLA Ops:
  0.6 0.0 copy-start
  0.7 1.4 dynamic_slice.7
  2.0 0.0 copy-done
  2.0 0.6 constant_dynamic-slice_fusion.taps
  2.6 0.0 copy-start.1
  2.6 190.5 %layer_group.1 = (bf16[256,2048]{1,0:T(8,128)(2,1)}, bf16[256,2048]{1,0:T(8,128)(2,1)}, bf16[2048,128]{1,0:T(8,128)(2,1)}) custom-call(bf16[256,2048]{1,0:T(8,128)(2,1)} %x0.1, bf16[256,2048]{1,0:T(8,128)(2,1)} %x1.1, bf16[256,2048]{1,0:T(8,128)(2,1)} %x2.1, bf16[128,2048]{1,0:T(8,128)(2,1)} %wg.1, bf16[128,2048]{1,0:T(8,128)(2,1)} %wu.1, ...), custom_call_target="tpu_custom_call" | custom-call | tf_op jit(solution)/shard_map/layer_group/pallas_call | solution.py:369
  193.1 0.0 copy-done.1
  193.1 0.0 copy-start.3
  193.1 2.2 %convert_add_fusion = f32[2048,128]{1,0:T(8,128)} fusion(f32[2048,128]{1,0:T(8,128)S(1)} %copy-done.1, bf16[2048,128]{1,0:T(8,128)(2,1)} %get-tuple-element.8), kind=kLoop, calls=%fused_computation | loop fusion | flops 524288 | bytes 2621440 | tf_op jit(solution)/shard_map/add | solution.py:472
  195.3 0.0 copy-done.3
  195.3 0.0 copy-start.2
  195.3 1.0 copy.14
  196.3 0.6 copy-done.2
  196.9 1.0 copy.15
Async XLA Ops:
  0.6 1.4 copy-start
  2.6 190.5 %copy-start.1 = (f32[2048,128]{1,0:T(8,128)S(1)}, f32[2048,128]{1,0:T(8,128)}, u32[]{:S(2)}) copy-start(f32[2048,128]{1,0:T(8,128)} %param.17) | copy-start | bytes 3145732
  193.1 2.2 %copy-start.3 = (bf16[256,2048]{1,0:T(8,128)(2,1)S(1)}, bf16[256,2048]{1,0:T(8,128)(2,1)}, u32[]{:S(2)}) copy-start(bf16[256,2048]{1,0:T(8,128)(2,1)} %get-tuple-element.12) | copy-start | bytes 3145732
  195.3 1.6 copy-start.2
